TPU v7x, 32 devices: a whole 2x2x4 slice. The times are simulated.
32 devices in a mesh: sp: 8 (over z, x), dp: 4 (over y, core).
Axes of the slice: x: 2, y: 2, z: 4, core: 2. Of those that a mesh axis runs over, the one named last changes fastest.
Arguments:
- inputs: bfloat16 [1536, 2048], P('sp'), may hold values from -6 to 6
- w_query: bfloat16 [2048, 2048], P('dp'), may hold values from -0.125 to 0.125
- w_key: bfloat16 [1024, 2048], P('dp'), may hold values from -0.125 to 0.125
- w_value: bfloat16 [1024, 2048], P('dp'), may hold values from -0.125 to 0.125
- query_gain: float32 [64], replicated, may hold values from 0.6 to 7
- key_gain: float32 [64], replicated, may hold values from 0.6 to 7
- grad_out: bfloat16 [1536, 2048], P('sp', 'dp'), may hold values from -6 to 6
Outputs:
- d_inputs: bfloat16 [1536, 2048], P('sp', 'dp')
- grad_wq: float32 [2048, 2048], P('dp')
- grad_wk: float32 [1024, 2048], P('dp')
- grad_wv: float32 [1024, 2048], P('dp')
All inputs are finite; a program needn't handle non-finite values.
Results may differ from a plain program's by a relative error of at most 0.019.
The roundings to bfloat16 on the way count: a program that leaves them out, or rounds other values in their place, can miss the bound.
Values may be sent and summed in bfloat16 or wider, within the bound.
No kernel may reach another device: no remote copies, remote signals or barrier semaphores. Data moves between devices by JAX's collectives and lax.ppermute only.
A program may use at most 64 MiB of HBM per device.

v0:
```python
import jax
import jax.numpy as jnp
from jax import lax
from jax.sharding import PartitionSpec as P

HEAD_WIDTH = 64
GRID_W = 64


norm_eps = 1e-06
axial_base = 10000.0


def rotation_tables(offset, count):
    positions = offset + jnp.arange(count, dtype=jnp.int32)
    grid_rows = (positions // GRID_W).astype(jnp.float32)
    grid_cols = (positions % GRID_W).astype(jnp.float32)
    quarter = HEAD_WIDTH // 4
    freqs_axis = axial_base ** (-jnp.arange(quarter, dtype=jnp.float32) / quarter)
    angle_rows = grid_rows[:, None] * freqs_axis[None, :]
    angle_cols = grid_cols[:, None] * freqs_axis[None, :]
    cosine = jnp.concatenate(
        [jnp.cos(angle_rows), jnp.cos(angle_rows), jnp.cos(angle_cols), jnp.cos(angle_cols)], axis=1
    )
    sine = jnp.concatenate(
        [jnp.sin(angle_rows), jnp.sin(angle_rows), jnp.sin(angle_cols), jnp.sin(angle_cols)], axis=1
    )
    return (cosine, sine)


def quarter_turn(values):
    quarter = HEAD_WIDTH // 4
    return jnp.concatenate(
        [
            -values[..., quarter : 2 * quarter],
            values[..., :quarter],
            -values[..., 3 * quarter :],
            values[..., 2 * quarter : 3 * quarter],
        ],
        axis=-1,
    )


def quarter_back(values):
    quarter = HEAD_WIDTH // 4
    return jnp.concatenate(
        [
            values[..., quarter : 2 * quarter],
            -values[..., :quarter],
            values[..., 3 * quarter :],
            -values[..., 2 * quarter : 3 * quarter],
        ],
        axis=-1,
    )


def rotate(values, cosine, sine):
    return values * cosine + quarter_turn(values) * sine


def rotate_back(grads, cosine, sine):
    return grads * cosine + quarter_back(grads * sine)


def head_norm(raw):
    scale_inv = lax.rsqrt(jnp.mean(raw * raw, axis=-1, keepdims=True) + norm_eps)
    return (raw * scale_inv, scale_inv)


def head_norm_back(grads, normed, scale_inv, gain):
    scaled = grads * gain
    return scale_inv * (scaled - normed * jnp.mean(scaled * normed, axis=-1, keepdims=True))


def body(inputs, w_query, w_key, w_value, query_gain, key_gain, grad_out):
    tok_rows = inputs.shape[0]
    local_query = w_query.shape[0] // HEAD_WIDTH
    local_keys = w_key.shape[0] // HEAD_WIDTH
    group = local_query // local_keys
    key_width = local_keys * HEAD_WIDTH
    scale = HEAD_WIDTH ** (-0.5)
    contract = (((1,), (1,)), ((), ()))
    leading = (((0,), (0,)), ((), ()))
    offset = lax.axis_index("sp") * tok_rows
    cosine, sine = rotation_tables(offset, tok_rows)
    cos_wide = cosine[:, None, :]
    sin_wide = sine[:, None, :]
    q_raw = lax.dot_general(inputs, w_query, contract, preferred_element_type=jnp.float32).astype(
        jnp.bfloat16
    )
    w_pair = jnp.concatenate([w_key, w_value], axis=0)
    kv_raw = lax.dot_general(inputs, w_pair, contract, preferred_element_type=jnp.float32).astype(
        jnp.bfloat16
    )
    q_wide = (
        lax.optimization_barrier(q_raw)
        .astype(jnp.float32)
        .reshape(tok_rows, local_query, HEAD_WIDTH)
    )
    k_wide = (
        lax.optimization_barrier(kv_raw[:, :key_width])
        .astype(jnp.float32)
        .reshape(tok_rows, local_keys, HEAD_WIDTH)
    )
    q_normed, q_inv = head_norm(q_wide)
    k_normed, k_inv = head_norm(k_wide)
    q_rot = rotate(q_normed * query_gain, cos_wide, sin_wide).astype(jnp.bfloat16)
    k_rot = rotate(k_normed * key_gain, cos_wide, sin_wide).astype(jnp.bfloat16)
    kv_rot = jnp.concatenate([k_rot.reshape(tok_rows, key_width), kv_raw[:, key_width:]], axis=1)
    kv_every = lax.all_gather(kv_rot, "sp", axis=0, tiled=True)
    seq_rows = kv_every.shape[0]
    keys_every = kv_every[:, :key_width]
    values_every = kv_every[:, key_width:]
    grad_query = []
    log_totals = []
    deltas = []
    key_terms = [jnp.zeros((seq_rows, HEAD_WIDTH), jnp.float32) for slot in range(local_keys)]
    value_terms = [jnp.zeros((seq_rows, HEAD_WIDTH), jnp.float32) for slot in range(local_keys)]
    for member in range(local_query):
        kv_index = member // group
        query_head = q_rot[:, member, :]
        key_head = keys_every[:, kv_index * HEAD_WIDTH : (kv_index + 1) * HEAD_WIDTH]
        value_head = values_every[:, kv_index * HEAD_WIDTH : (kv_index + 1) * HEAD_WIDTH]
        grad_head = grad_out[:, member * HEAD_WIDTH : (member + 1) * HEAD_WIDTH]
        scores = (
            lax.dot_general(query_head, key_head, contract, preferred_element_type=jnp.float32)
            * scale
        )
        maxima = jnp.max(scores, axis=1, keepdims=True)
        log_total = maxima + jnp.log(jnp.sum(jnp.exp(scores - maxima), axis=1, keepdims=True))
        prob_exact = jnp.exp(scores - log_total)
        prob_half = prob_exact.astype(jnp.bfloat16)
        attn_rows = jnp.dot(prob_half, value_head, preferred_element_type=jnp.float32).astype(
            jnp.bfloat16
        )
        attn_wide = lax.optimization_barrier(attn_rows).astype(jnp.float32)
        delta_rows = jnp.sum(grad_head.astype(jnp.float32) * attn_wide, axis=1, keepdims=True)
        dprob = lax.dot_general(grad_head, value_head, contract, preferred_element_type=jnp.float32)
        dscore = (prob_exact * (dprob - delta_rows)).astype(jnp.bfloat16)
        grad_query.append(jnp.dot(dscore, key_head, preferred_element_type=jnp.float32) * scale)
        log_totals.append(log_total)
        deltas.append(delta_rows)
        value_terms[kv_index] = value_terms[kv_index] + lax.dot_general(
            prob_half, grad_head, leading, preferred_element_type=jnp.float32
        )
        key_terms[kv_index] = (
            key_terms[kv_index]
            + lax.dot_general(dscore, query_head, leading, preferred_element_type=jnp.float32)
            * scale
        )
    gradient_query_rotated = jnp.stack(grad_query, axis=1)
    partial_sums = jnp.concatenate(key_terms + value_terms, axis=1)
    own_grads = lax.psum_scatter(partial_sums, "sp", scatter_dimension=0, tiled=True)
    gradient_key_rotated = own_grads[:, :key_width].reshape(tok_rows, local_keys, HEAD_WIDTH)
    grad_q = head_norm_back(
        rotate_back(gradient_query_rotated, cos_wide, sin_wide), q_normed, q_inv, query_gain
    )
    grad_q = grad_q.reshape(tok_rows, local_query * HEAD_WIDTH).astype(jnp.bfloat16)
    grad_k = head_norm_back(
        rotate_back(gradient_key_rotated, cos_wide, sin_wide), k_normed, k_inv, key_gain
    )
    grad_kv = jnp.concatenate(
        [
            grad_k.reshape(tok_rows, key_width).astype(jnp.bfloat16),
            own_grads[:, key_width:].astype(jnp.bfloat16),
        ],
        axis=1,
    )
    head_part = jnp.dot(grad_q, w_query, preferred_element_type=jnp.float32)
    head_part = head_part + jnp.dot(grad_kv, w_pair, preferred_element_type=jnp.float32)
    d_inputs = lax.psum_scatter(
        head_part.astype(jnp.bfloat16), "dp", scatter_dimension=1, tiled=True
    )
    grad_wq = lax.dot_general(grad_q, inputs, leading, preferred_element_type=jnp.float32)
    grad_wkv = lax.dot_general(grad_kv, inputs, leading, preferred_element_type=jnp.float32)
    grad_wq, grad_wkv = lax.psum((grad_wq, grad_wkv), "sp")
    return (d_inputs, grad_wq, grad_wkv[:key_width], grad_wkv[key_width:])


def solution(mesh):
    return jax.shard_map(
        body,
        mesh=mesh,
        in_specs=(
            P("sp", None),
            P("dp", None),
            P("dp", None),
            P("dp", None),
            P(),
            P(),
            P("sp", "dp"),
        ),
        out_specs=(P("sp", "dp"), P("dp", None), P("dp", None), P("dp", None)),
        check_vma=False,
    )
```

profile of v0, /device:TPU:0, one launch (start us, length us, event | category | flops | bytes accessed | tf_op | source)
XLA Modules:
  0.0 498.9 jit_solution(4581374337283304342)
XLA Ops:
  16.6 1.7 copy.97
  21.3 1.6 pad_maximum_fusion.1
  22.9 1.5 convolution_convert_fusion.1
  34.6 35.3 %all-gather.2.cloned.1.call-done = bf16[1536,512]{1,0:T(8,128)(2,1)} async-done(((bf16[192,512]{1,0:T(8,128)(2,1)}), bf16[1536,512]{1,0:T(8,128)(2,1)}) %all-gather.2.cloned.1.call-update) | async-done | bytes 1572880 | tf_op jit(solution)/shard_map/all_gather | solution.py:110
  69.9 1.6 fusion.148
  100.5 3.5 copy.117
  106.2 2.0 copy.109
  108.3 1.6 fusion.53
  109.9 1.6 fusion.51
  111.5 1.7 fusion.49
  116.6 1.6 multiply_reduce_fusion
  118.2 2.0 copy.106
  123.2 2.8 fusion.156
  126.0 51.0 %reduce-scatter.7.cloned.1.call-done = f32[192,512]{1,0:T(8,128)} async-done(((f32[1536,512]{1,0:T(8,128)}), f32[192,512]{1,0:T(8,128)}) %reduce-scatter.7.cloned.1.call-update) | async-done | bytes 393232 | tf_op jit(solution)/shard_map/reduce_scatter | solution.py:153
  177.0 1.6 slice.233
  178.6 1.8 copy.112
  181.5 1.6 pad_maximum_fusion
  183.1 1.8 copy.113
  185.7 1.7 copy.114
  190.3 2.7 fusion.96
  196.3 266.0 %all-reduce.3.cloned.1.call-done = (f32[512,2048]{1,0:T(8,128)}, f32[512,2048]{1,0:T(8,128)}) async-done(((f32[512,2048]{1,0:T(8,128)}, f32[512,2048]{1,0:T(8,128)}), (f32[512,2048]{1,0:T(8,128)}, f32[512,2048]{1,0:T(8,128)})) %all-reduce.3.cloned.1.call-update) | async-done | bytes 8388624 | tf_op jit(solution)/shard_map/psum | solution.py:176
  462.3 4.7 fusion.142
  467.0 20.6 %reduce-scatter.5.cloned.1.call-done = bf16[192,512]{1,0:T(8,128)(2,1)} async-done(((bf16[192,2048]{1,0:T(8,128)(2,1)}), bf16[192,512]{1,0:T(8,128)(2,1)}) %reduce-scatter.5.cloned.1.call-update) | async-done | bytes 196624 | tf_op jit(solution)/shard_map/reduce_scatter | solution.py:171
  487.7 4.7 copy.144
  (230 shorter events, 67.6 us)
Async XLA Ops:
  7.2 15.8 %copy-start = (bf16[512,2048]{1,0:T(8,128)(2,1)S(1)}, bf16[512,2048]{1,0:T(8,128)(2,1)}, u32[]{:S(2)}) copy-start(bf16[512,2048]{1,0:T(8,128)(2,1)} %param.8) | copy-start | bytes 6291460
  7.2 62.7 %all-gather.2.cloned.1.call-start = ((), (), s32[]{:S(2)}) async-start(), calls=%async_computation.2 | async-start | bytes 1769472 | tf_op jit(solution)/shard_map/all_gather | solution.py:110
  8.1 12.0 %copy-start.43 = (f32[256]{0:T(256)}, f32[256]{0:T(256)S(1)}, u32[]{:S(2)}) copy-start(f32[256]{0:T(256)S(1)} %mul.354) | copy-start | bytes 3076
  9.0 107.1 %copy-start.29 = (f32[192,64]{0,1:T(8,128)}, f32[192,64]{0,1:T(8,128)S(1)}, u32[]{:S(2)}) copy-start(f32[192,64]{0,1:T(8,128)S(1)} %pad_maximum_fusion.5) | copy-start | bytes 147460
  9.1 11.0 %copy-start.25 = (f32[192,256]{1,0:T(8,128)}, f32[192,256]{1,0:T(8,128)S(1)}, u32[]{:S(2)}) copy-start(f32[192,256]{1,0:T(8,128)S(1)} %copy.96) | copy-start | bytes 589828
  11.9 3.1 copy-start.48
  14.9 3.5 copy-start.21
  20.1 2.7 copy-start.27
  22.9 154.1 %reduce-scatter.7.cloned.1.call-start = ((), (), s32[]{:S(2)}) async-start(), calls=%async_computation.4 | async-start | bytes 3538944 | tf_op jit(solution)/shard_map/reduce_scatter | solution.py:153
  24.5 9.1 %copy-start.45 = (f32[64]{0:T(128)S(1)}, f32[64]{0:T(128)}, u32[]{:S(2)}) copy-start(f32[64]{0:T(128)} %param.11) | copy-start | bytes 772
  69.9 1.9 copy-start.1
  94.9 2.1 copy-start.12
  104.0 358.3 %all-reduce.3.cloned.1.call-start = ((), (), s32[]{:S(2)}) async-start(), calls=%async_computation.5 | async-start | bytes 16777216 | tf_op jit(solution)/shard_map/psum | solution.py:176
  108.3 3.2 copy-start.2
  109.9 3.3 copy-start.17
  111.5 2.2 copy-start.9
  118.1 3.7 copy-start.47
  126.0 55.5 %copy-start.22 = (f32[192,256]{0,1:T(8,128)S(1)}, f32[192,256]{0,1:T(8,128)}, u32[]{:S(2)}) copy-start(f32[192,256]{0,1:T(8,128)} %copy-done.21) | copy-start | bytes 589828
  126.0 55.5 %copy-start.49 = (f32[64]{0:T(128)S(1)}, f32[64]{0:T(128)}, u32[]{:S(2)}) copy-start(f32[64]{0:T(128)} %param.12) | copy-start | bytes 772
  181.5 6.8 %copy-start.26 = (f32[192,256]{1,0:T(8,128)S(1)}, f32[192,256]{1,0:T(8,128)}, u32[]{:S(2)}) copy-start(f32[192,256]{1,0:T(8,128)} %copy-done.25) | copy-start | bytes 589828
  181.5 6.8 %copy-start.44 = (f32[256]{0:T(256)S(1)}, f32[256]{0:T(256)}, u32[]{:S(2)}) copy-start(f32[256]{0:T(256)} %copy-done.43) | copy-start | bytes 3076
  183.1 5.2 %copy-start.28 = (f32[192,256]{1,0:T(8,128)S(1)}, f32[192,256]{1,0:T(8,128)}, u32[]{:S(2)}) copy-start(f32[192,256]{1,0:T(8,128)} %copy-done.27) | copy-start | bytes 589828
  193.1 294.6 %reduce-scatter.5.cloned.1.call-start = ((), (), s32[]{:S(2)}) async-start(), calls=%async_computation.3 | async-start | bytes 983040 | tf_op jit(solution)/shard_map/reduce_scatter | solution.py:171
  193.1 1.6 copy-start.20
  (30 other events, 28.9 us)
Sparse Core Ops, SparseCore 0:
  23.0 46.8 all-gather.1
  104.2 72.8 reduce-scatter.6
  193.2 269.0 all-reduce.2
  465.3 22.3 reduce-scatter.4
where the time goes:
time: 500 us; the launch traced here: 499 us
  waiting for transfers between devices  373 us (75%)
  local copies, waits for them, and re-layouts  54.1 us (11%)
  matrix products  40.2 us (8%)
  other arithmetic  16.9 us (3%)
  between operations  14.6 us (3%)
    psum x1, waiting for transfers between devices, body(): grad_wq, grad_wkv = lax.psum((grad_wq, grad_wkv), 'sp')  266 us
    reduce_scatter x1, waiting for transfers between devices, body(): lax.psum_scatter(partial_sums, 'sp', scatter_dimension=0, tiled=True)  51 us
    all_gather x1, waiting for transfers between devices, body(): kv_every = lax.all_gather(kv_rot, 'sp', axis=0, tiled=True)  35.3 us
    unnamed x112, local copies, waits for them, and re-layouts  26.3 us
    reduce_scatter x1, waiting for transfers between devices, body(): lax.psum_scatter(head_part.astype(jnp.bfloat16), 'dp', scatter_dimension=...  20.6 us
  transfers between devices with their start and end apart: 4, of which 4 were waited for; matrix products, arithmetic and copies ran while one was open for 8% of the time, Pallas kernels for 0%

commit v1 on v0

--- a/solution.py
+++ b/solution.py
@@ -1,6 +1,8 @@
 import jax
 import jax.numpy as jnp
 from jax import lax
+from jax.experimental import pallas as pl
+from jax.experimental.pallas import tpu as pltpu
 from jax.sharding import PartitionSpec as P
 
 HEAD_WIDTH = 64
@@ -177,9 +179,270 @@
     return (d_inputs, grad_wq, grad_wkv[:key_width], grad_wkv[key_width:])
 
 
+def ring_order(index, count):
+    return jnp.where(index < count // 2, 2 * index, 2 * (count - 1 - index) + 1)
+
+
+def ring_place(device, count):
+    return jnp.where(device % 2 == 0, device // 2, count - 1 - device // 2)
+
+
+def ring_steps(block, me, count):
+    order = list(range(0, count, 2)) + list(range(count - 1, 0, -2))
+    ahead = [(order[i], order[(i + 1) % count]) for i in range(count)]
+    behind = [(b, a) for a, b in ahead]
+    place = ring_place(me, count)
+    yield me, block
+    first = second = block
+    for step in range(1, count // 2 + 1):
+        first = lax.ppermute(first, "sp", ahead)
+        if step < count // 2:
+            second = lax.ppermute(second, "sp", behind)
+        yield ring_order((place - step) % count, count), first
+        if step < count // 2:
+            yield ring_order((place + step) % count, count), second
+
+
+def dot_nt(a, b):
+    return lax.dot_general(a, b, (((1,), (1,)), ((), ())), preferred_element_type=jnp.float32)
+
+
+def dot_nn(a, b):
+    return jnp.dot(a, b, preferred_element_type=jnp.float32)
+
+
+def project_kernel(x_ref, wq_ref, wk_ref, wv_ref, grad_ref, out_ref):
+    heads = out_ref.shape[0]
+    group = wq_ref.shape[0] // wk_ref.shape[0]
+    x = x_ref[...]
+    q = dot_nt(x, wq_ref[...]).astype(jnp.bfloat16)
+    k = dot_nt(x, wk_ref[...]).astype(jnp.bfloat16)
+    v = dot_nt(x, wv_ref[...]).astype(jnp.bfloat16)
+    grad = grad_ref[...]
+
+    def head(values, index):
+        return values[:, index * HEAD_WIDTH : (index + 1) * HEAD_WIDTH]
+
+    for h in range(heads):
+        out_ref[h] = jnp.concatenate(
+            [head(q, h), head(k, h // group), head(grad, h), head(v, h // group)], axis=1
+        )
+
+
+def turn_rows(values):
+    q = HEAD_WIDTH // 4
+    return jnp.concatenate(
+        [-values[q : 2 * q], values[:q], -values[3 * q :], values[2 * q : 3 * q]], axis=0
+    )
+
+
+def back_rows(values):
+    q = HEAD_WIDTH // 4
+    return jnp.concatenate(
+        [values[q : 2 * q], -values[:q], values[3 * q :], -values[2 * q : 3 * q]], axis=0
+    )
+
+
+def norm_rows(raw):
+    inv = lax.rsqrt(jnp.mean(raw * raw, axis=0, keepdims=True) + norm_eps)
+    return raw * inv, inv
+
+
+def norm_back_rows(grads, normed, inv, gain):
+    scaled = grads * gain
+    return inv * (scaled - normed * jnp.mean(scaled * normed, axis=0, keepdims=True))
+
+
+def attention_kernel(
+    x_ref, cos_ref, sin_ref, qg_ref, kg_ref, gq_ref, dkv_ref, kn_ref, ki_ref, q_s, go_s, k_s, qn_s, qi_s, dq_s
+):
+    width = HEAD_WIDTH
+    seq = x_ref.shape[0]
+    scale = width ** (-0.5)
+    xt = x_ref[...].T
+    cosine = cos_ref[...]
+    sine = sin_ref[...]
+    qn, qi = norm_rows(xt[:width].astype(jnp.float32))
+    kn, ki = norm_rows(xt[width : 2 * width].astype(jnp.float32))
+    qn_s[...] = qn
+    qi_s[...] = qi
+    kn_ref[...] = kn
+    ki_ref[...] = jnp.broadcast_to(ki, ki_ref.shape)
+    qg = qn * qg_ref[...]
+    kg = kn * kg_ref[...]
+    q_s[...] = (qg * cosine + turn_rows(qg) * sine).astype(jnp.bfloat16)
+    kt = (kg * cosine + turn_rows(kg) * sine).astype(jnp.bfloat16)
+    go_s[...] = xt[2 * width : 3 * width]
+    vt = xt[3 * width :]
+    k_s[:width] = kt
+    k_s[width:] = vt
+    rows = k_s[...].T
+    k_rows = rows[:, :width]
+    v_rows = rows[:, width:]
+    dkv_ref[...] = jnp.zeros_like(dkv_ref)
+    block = 256
+
+    def step(i, carry):
+        at = pl.ds(pl.multiple_of(i * block, block), block)
+        q = q_s[:, at]
+        go = go_s[:, at]
+        scores = dot_nn(k_rows, q) * scale
+        maxima = jnp.max(scores, axis=0, keepdims=True)
+        weights = jnp.exp(scores - maxima)
+        prob = weights * (1.0 / jnp.sum(weights, axis=0, keepdims=True))
+        half = prob.astype(jnp.bfloat16)
+        attn = dot_nn(vt, half).astype(jnp.bfloat16)
+        delta = jnp.sum(go.astype(jnp.float32) * attn.astype(jnp.float32), axis=0, keepdims=True)
+        dprob = dot_nn(v_rows, go)
+        dscore = (prob * (dprob - delta)).astype(jnp.bfloat16)
+        dq_s[:, at] = dot_nn(kt, dscore) * scale
+        dkv_ref[:width] += dot_nt(q, dscore) * scale
+        dkv_ref[width:] += dot_nt(go, half)
+        return carry
+
+    lax.fori_loop(0, seq // block, step, 0)
+    dq = dq_s[...]
+    back = dq * cosine + back_rows(dq * sine)
+    gq_ref[...] = norm_back_rows(back, qn_s[...], qi_s[...], qg_ref[...]).astype(jnp.bfloat16)
+
+
+def key_kernel(part_ref, own_ref, other_ref, kn_ref, ki_ref, cos_ref, sin_ref, kg_ref, out_ref):
+    width = HEAD_WIDTH
+    total = own_ref[...] + other_ref[...]
+    dk = total[:width]
+    back = dk * cos_ref[...] + back_rows(dk * sin_ref[...])
+    out_ref[:width] = norm_back_rows(back, kn_ref[...], ki_ref[:1], kg_ref[...]).astype(jnp.bfloat16)
+    out_ref[width:] = total[width:].astype(jnp.bfloat16)
+
+
+def head_body(inputs, w_query, w_key, w_value, query_gain, key_gain, grad_out):
+    count = lax.axis_size("sp")
+    cores = lax.axis_size("dp")
+    tok, width = inputs.shape
+    seq = tok * count
+    heads = w_query.shape[0] // HEAD_WIDTH
+    keys = w_key.shape[0] // HEAD_WIDTH
+    half_w = width // 2
+    half_s = seq // 2
+    me = lax.axis_index("sp")
+    side = lax.axis_index("dp") % 2
+    bf16, f32 = jnp.bfloat16, jnp.float32
+    struct = jax.ShapeDtypeStruct
+
+    blocks = pl.pallas_call(
+        project_kernel, out_shape=struct((heads, tok, 4 * HEAD_WIDTH), bf16), name="project"
+    )(inputs, w_query, w_key, w_value, grad_out)
+    gathered = lax.all_to_all(
+        blocks.reshape(heads * tok, 4 * HEAD_WIDTH), "sp", split_axis=0, concat_axis=0, tiled=True
+    )
+
+    mine = lax.dynamic_slice(inputs, (0, side * half_w), (tok, half_w))
+    x_half = jnp.zeros((seq, half_w), bf16)
+    for source, piece in ring_steps(mine, me, count):
+        x_half = lax.dynamic_update_slice(x_half, piece, (source * tok, 0))
+    x_other = lax.ppermute(x_half, "dp", [(i, i ^ 1) for i in range(cores)])
+
+    cosine, sine = rotation_tables(0, seq)
+    cosine, sine = cosine.T, sine.T
+    qg = query_gain[:, None]
+    kg = key_gain[:, None]
+    vmem = pltpu.VMEM
+    gq, dkv, kn, ki = pl.pallas_call(
+        attention_kernel,
+        out_shape=(
+            struct((HEAD_WIDTH, seq), bf16),
+            struct((2 * HEAD_WIDTH, seq), f32),
+            struct((HEAD_WIDTH, seq), f32),
+            struct((8, seq), f32),
+        ),
+        scratch_shapes=[
+            vmem((HEAD_WIDTH, seq), bf16),
+            vmem((HEAD_WIDTH, seq), bf16),
+            vmem((2 * HEAD_WIDTH, seq), bf16),
+            vmem((HEAD_WIDTH, seq), f32),
+            vmem((1, seq), f32),
+            vmem((HEAD_WIDTH, seq), f32),
+        ],
+        name="attention",
+    )(gathered, cosine, sine, qg, kg)
+
+    part = me % 2
+    away = lax.dynamic_slice(dkv, (0, (1 - part) * half_s), (2 * HEAD_WIDTH, half_s))
+    other = lax.ppermute(away, "sp", [(i, i ^ 1) for i in range(count)])
+
+    def at_part(rows):
+        return pl.BlockSpec((rows, half_s), lambda i, p: (0, p[0]))
+
+    def whole(rows, cols):
+        return pl.BlockSpec((rows, cols), lambda i, p: (0, 0))
+
+    gkv = pl.pallas_call(
+        key_kernel,
+        out_shape=struct((2 * HEAD_WIDTH, half_s), bf16),
+        grid_spec=pltpu.PrefetchScalarGridSpec(
+            num_scalar_prefetch=1,
+            grid=(1,),
+            in_specs=[
+                at_part(2 * HEAD_WIDTH),
+                whole(2 * HEAD_WIDTH, half_s),
+                at_part(HEAD_WIDTH),
+                at_part(8),
+                at_part(HEAD_WIDTH),
+                at_part(HEAD_WIDTH),
+                whole(HEAD_WIDTH, 1),
+            ],
+            out_specs=whole(2 * HEAD_WIDTH, half_s),
+        ),
+        name="keys",
+    )(part.reshape(1).astype(jnp.int32), dkv, other, kn, ki, cosine, sine, kg)
+
+    gq_every = jnp.zeros((heads * HEAD_WIDTH, seq), bf16)
+    for source, piece in ring_steps(gq, me, count):
+        gq_every = lax.dynamic_update_slice(gq_every, piece, (source * HEAD_WIDTH, 0))
+    gk_every = jnp.zeros((keys * HEAD_WIDTH, seq), bf16)
+    gv_every = jnp.zeros((keys * HEAD_WIDTH, seq), bf16)
+    for source, piece in ring_steps(gkv, me, count):
+        where = (source // 2 * HEAD_WIDTH, source % 2 * half_s)
+        gk_every = lax.dynamic_update_slice(gk_every, piece[:HEAD_WIDTH], where)
+        gv_every = lax.dynamic_update_slice(gv_every, piece[HEAD_WIDTH:], where)
+
+    x_every = jnp.zeros((seq, width), bf16)
+    x_every = lax.dynamic_update_slice(x_every, x_half, (0, side * half_w))
+    x_every = lax.dynamic_update_slice(x_every, x_other, (0, (1 - side) * half_w))
+
+    leading = (((0,), (0,)), ((), ()))
+
+    def share(grads, weight):
+        own = lax.dynamic_slice(grads, (0, me * tok), (grads.shape[0], tok))
+        return lax.dot_general(own, weight, leading, preferred_element_type=f32)
+
+    head_part = share(gq_every, w_query) + share(gk_every, w_key) + share(gv_every, w_value)
+    shares = lax.all_to_all(
+        head_part.astype(bf16), "dp", split_axis=1, concat_axis=0, tiled=True
+    ).reshape(cores, tok, width // cores)
+    d_inputs = jnp.sum(shares.astype(f32), axis=0).astype(bf16)
+    return (
+        d_inputs,
+        dot_nn(gq_every, x_every),
+        dot_nn(gk_every, x_every),
+        dot_nn(gv_every, x_every),
+    )
+
+
+def choose(inputs, w_query, w_key, w_value, query_gain, key_gain, grad_out):
+    count = lax.axis_size("sp")
+    cores = lax.axis_size("dp")
+    heads = w_query.shape[0] // HEAD_WIDTH
+    keys = w_key.shape[0] // HEAD_WIDTH
+    seq = inputs.shape[0] * count
+    fits = heads == count and heads == 2 * keys and cores % 2 == 0 and seq % 256 == 0
+    run = head_body if fits else body
+    return run(inputs, w_query, w_key, w_value, query_gain, key_gain, grad_out)
+
+
 def solution(mesh):
     return jax.shard_map(
-        body,
+        choose,
         mesh=mesh,
         in_specs=(
             P("sp", None),

time: 500 us -> 167 us (0.33)
  waiting for transfers between devices: 373 us -> 43.1 us
  starting transfers between devices: 0.16 us -> 39.1 us
  Pallas kernels: 0 us -> 23.5 us
  local copies, waits for them, and re-layouts: 54.1 us -> 31.8 us
  matrix products: 40.2 us -> 23.2 us
  between operations: 14.6 us -> 0.96 us
  other arithmetic: 16.9 us -> 4.3 us
    psum x1 -> x0, waiting for transfers between devices: 266 us -> none  [body(): grad_wq, grad_wkv = lax.psum((grad_wq, grad_wkv), 'sp')]
    reduce_scatter x2 -> x0, waiting for transfers between devices: 71.6 us -> none  [the longest x1 51 us: body(): lax.psum_scatter(partial_sums, 'sp', scatter_dimension=0, tiled=True)]
    ppermute x0 -> x23, waiting for transfers between devices: none -> 37.1 us  [the longest x12 32.9 us: ring_steps(): first = lax.ppermute(first, 'sp', ahead)]
    all_gather x1 -> x0, waiting for transfers between devices: 35.3 us -> none  [body(): kv_every = lax.all_gather(kv_rot, 'sp', axis=0, tiled=True)]
    ppermute x0 -> x23, starting transfers between devices: none -> 28.3 us  [the longest x12 19.6 us: ring_steps(): first = lax.ppermute(first, 'sp', ahead)]
    unnamed x112 -> x26, local copies, waits for them, and re-layouts: 26.3 us -> 2.69 us
    pallas_call x0 -> x3, Pallas kernels: none -> 23.5 us  [the longest x1 16.5 us: head_body(): pl.pallas_call(attention_kernel, out_shape=(struct((HEAD_WIDTH, seq), bf1...]
    dynamic_update_slice x0 -> x27, local copies, waits for them, and re-layouts: none -> 20.6 us  [the longest x8 7.43 us: head_body(): lax.dynamic_update_slice(gq_every, piece, (source * HEAD_WIDTH, 0))]
  transfers between devices with their start and end apart: 4 -> 25, of which waited for: 4 -> 12; matrix products, arithmetic and copies ran while one was open for 8% -> 19% of each run, Pallas kernels for 0% -> 14%
where the time goes in v1:
time: 167 us; the launch traced here: 166 us
  waiting for transfers between devices  43.1 us (26%)
  starting transfers between devices  39.1 us (23%)
  local copies, waits for them, and re-layouts  31.8 us (19%)
  Pallas kernels  23.5 us (14%)
  matrix products  23.2 us (14%)
  other arithmetic  4.3 us (3%)
    ppermute x12, waiting for transfers between devices, ring_steps(): first = lax.ppermute(first, 'sp', ahead)  32.9 us
    dot_general x3, matrix products, dot_nn(): return jnp.dot(a, b, preferred_element_type=jnp.float32)  20.6 us
    ppermute x12, starting transfers between devices, ring_steps(): first = lax.ppermute(first, 'sp', ahead)  19.6 us
    pallas_call x1, Pallas kernels, head_body(): pl.pallas_call(attention_kernel, out_shape=(struct((HEAD_WIDTH, seq), bf1...  16.5 us
    ppermute x9, starting transfers between devices, ring_steps(): second = lax.ppermute(second, 'sp', behind)  7.52 us
    dynamic_update_slice x8, local copies, waits for them, and re-layouts, head_body(): lax.dynamic_update_slice(gq_every, piece, (source * HEAD_WIDTH, 0))  7.43 us
    all_to_all x1, starting transfers between devices, head_body(): lax.all_to_all(blocks.reshape(heads * tok, 4 * HEAD_WIDTH), 'sp', split_a...  6.38 us
    dynamic_update_slice x8, local copies, waits for them, and re-layouts, head_body(): x_half = lax.dynamic_update_slice(x_half, piece, (source * tok, 0))  6.04 us
  transfers between devices with their start and end apart: 25, of which 12 were waited for; matrix products, arithmetic and copies ran while one was open for 19% of the time, Pallas kernels for 14%

profile of v1, /device:TPU:0, one launch (start us, length us, event | category | flops | bytes accessed | tf_op | source)
XLA Modules:
  0.0 166.0 jit_solution(10298052152499902317)
XLA Ops:
  2.6 3.1 %collective-permute-start.15 = (bf16[192,1024]{1,0:T(8,128)(2,1)}, bf16[192,1024]{1,0:T(8,128)(2,1)}, u32[]{:S(2)}, u32[]{:S(2)}) collective-permute-start(bf16[192,1024]{1,0:T(8,128)(2,1)} %get-tuple-element.13), channel_id=1, source_target_pairs={{0,8},{8,16},{16,24},{24,28},{28,20},{20,12},{12,4},{4,0},{1,9},{9... | collective-permute-start | bytes 1179656 | tf_op jit(solution)/shard_map/ppermute | solution.py:198
  5.7 4.9 %project.1 = bf16[8,192,256]{2,1,0:T(8,128)(2,1)} custom-call(bf16[192,2048]{1,0:T(8,128)(2,1)} %x_ref.1, bf16[512,2048]{1,0:T(8,128)(2,1)} %wq_ref.1, bf16[256,2048]{1,0:T(8,128)(2,1)} %wk_ref.1, bf16[256,2048]{1,0:T(8,128)(2,1)} %wv_ref.1, bf16[192,512]{1,0:T(8,128)(2,1)} %grad_ref.1), custom_call_target="tpu_custom_call" | custom-call | tf_op jit(solution)/shard_map/project/pallas_call | solution.py:332
  10.6 6.4 %all-to-all-start = ((bf16[8,192,256]{2,1,0:T(8,128)(2,1)}), bf16[8,192,256]{2,1,0:T(8,128)(2,1)}, u32[]{:S(2)}, u32[]{:S(2)}) async-start(bf16[8,192,256]{2,1,0:T(8,128)(2,1)} %project.1), calls=%async_computation | async-start | bytes 1572864 | tf_op jit(solution)/shard_map/all_to_all | solution.py:335
  17.8 2.1 %collective-permute-start.17 = (bf16[192,1024]{1,0:T(8,128)(2,1)}, bf16[192,1024]{1,0:T(8,128)(2,1)}, u32[]{:S(2)}, u32[]{:S(2)}) collective-permute-start(bf16[192,1024]{1,0:T(8,128)(2,1)} %collective-permute-done.15), channel_id=1, source_target_pairs={{0,8},{8,16},{16,24},{24,28},{28,20},{20,12},{12,4},{4,0},{1,9},{9... | collective-permute-start | bytes 1179656 | tf_op jit(solution)/shard_map/ppermute | solution.py:198
  22.9 15.0 %collective-permute-done.17 = bf16[192,1024]{1,0:T(8,128)(2,1)} collective-permute-done((bf16[192,1024]{1,0:T(8,128)(2,1)}, bf16[192,1024]{1,0:T(8,128)(2,1)}, u32[]{:S(2)}, u32[]{:S(2)}) %collective-permute-start.17) | collective-permute-done | bytes 393248 | tf_op jit(solution)/shard_map/ppermute | solution.py:198
  37.8 5.6 %collective-permute-start.19 = (bf16[192,1024]{1,0:T(8,128)(2,1)}, bf16[192,1024]{1,0:T(8,128)(2,1)S(1)}, u32[]{:S(2)}, u32[]{:S(2)}) collective-permute-start(bf16[192,1024]{1,0:T(8,128)(2,1)} %collective-permute-done.17), channel_id=1, source_target_pairs={{0,8},{8,16},{16,24},{24,28},{28,20},{20,12},{12,4},{4,0},{1,9},{9... | collective-permute-start | bytes 1179656 | tf_op jit(solution)/shard_map/ppermute | solution.py:198
  47.7 3.9 %collective-permute-done.19 = bf16[192,1024]{1,0:T(8,128)(2,1)S(1)} collective-permute-done((bf16[192,1024]{1,0:T(8,128)(2,1)}, bf16[192,1024]{1,0:T(8,128)(2,1)S(1)}, u32[]{:S(2)}, u32[]{:S(2)}) %collective-permute-start.19) | collective-permute-done | bytes 393248 | tf_op jit(solution)/shard_map/ppermute | solution.py:198
  51.5 2.5 %collective-permute-start.21 = (bf16[192,1024]{1,0:T(8,128)(2,1)S(1)}, bf16[192,1024]{1,0:T(8,128)(2,1)}, u32[]{:S(2)}, u32[]{:S(2)}) collective-permute-start(bf16[192,1024]{1,0:T(8,128)(2,1)S(1)} %collective-permute-done.19), channel_id=1, source_target_pairs={{0,8},{8,16},{16,24},{24,28},{28,20},{20,12},{12,4},{4,0},{1,9},{9... | collective-permute-start | bytes 1179656 | tf_op jit(solution)/shard_map/ppermute | solution.py:198
  55.5 16.5 %attention.1 = (bf16[64,1536]{1,0:T(8,128)(2,1)}, f32[128,1536]{1,0:T(8,128)}, f32[64,1536]{1,0:T(8,128)}, f32[8,1536]{1,0:T(8,128)}) custom-call(bf16[1536,256]{1,0:T(8,128)(2,1)} %bitcast.x_ref, f32[64,1536]{1,0:T(8,128)} %maximum_bitcast_fusion.cos_ref, f32[64,1536]{1,0:T(8,128)} %maximum_bitcast_fusion.1.sin_ref, f32[64,1]{1,0:T(8,128)} %copy.14.qg_ref, ...), custom_call_target="tpu_custom_call" | custom-call | tf_op jit(solution)/shard_map/attention/pallas_call | solution.py:350
  85.3 2.8 %collective-permute-done.7.other_ref = f32[128,768]{1,0:T(8,128)S(1)} collective-permute-done((f32[128,768]{1,0:T(8,128)S(1)}, f32[128,768]{1,0:T(8,128)S(1)}, u32[]{:S(2)}, u32[]{:S(2)}) %collective-permute-start.7) | collective-permute-done | bytes 393248 | tf_op jit(solution)/shard_map/ppermute | solution.py:371
  88.9 2.1 %keys.1 = bf16[128,768]{1,0:T(8,128)(2,1)} custom-call(s32[1]{0:T(128)} %bitcast.5.part_ref, f32[128,1536]{1,0:T(8,128)} %get-tuple-element.9.own_ref, f32[128,768]{1,0:T(8,128)} %copy-done.9, f32[64,1536]{1,0:T(8,128)} %get-tuple-element.10.kn_ref, f32[8,1536]{1,0:T(8,128)} %get-tuple-element.11.ki_ref, f32[64,1536]{1,0:T(8,128)} %maximum_bitcast_fusion.cos_ref, ...), custom_call_target="tpu_custom_call" | custom-call | tf_op jit(solution)/shard_map/keys/pallas_call | solution.py:379
  91.0 2.0 %collective-permute-start.9 = (bf16[128,768]{1,0:T(8,128)(2,1)}, bf16[128,768]{1,0:T(8,128)(2,1)S(1)}, u32[]{:S(2)}, u32[]{:S(2)}) collective-permute-start(bf16[128,768]{1,0:T(8,128)(2,1)} %keys.1), channel_id=1, source_target_pairs={{8,0},{16,8},{24,16},{28,24},{20,28},{12,20},{4,12},{0,4},{9,1},{1... | collective-permute-start | bytes 589832 | tf_op jit(solution)/shard_map/ppermute | solution.py:200
  94.0 2.1 %collective-permute-start.5 = (bf16[64,1536]{1,0:T(8,128)(2,1)S(1)}, bf16[64,1536]{1,0:T(8,128)(2,1)S(1)}, u32[]{:S(2)}, u32[]{:S(2)}) collective-permute-start(bf16[64,1536]{1,0:T(8,128)(2,1)S(1)} %collective-permute-done.3), channel_id=1, source_target_pairs={{8,0},{16,8},{24,16},{28,24},{20,28},{12,20},{4,12},{0,4},{9,1},{1... | collective-permute-start | bytes 589832 | tf_op jit(solution)/shard_map/ppermute | solution.py:200
  110.2 2.8 %collective-permute-done.12 = bf16[128,768]{1,0:T(8,128)(2,1)S(1)} collective-permute-done((bf16[128,768]{1,0:T(8,128)(2,1)S(1)}, bf16[128,768]{1,0:T(8,128)(2,1)S(1)}, u32[]{:S(2)}, u32[]{:S(2)}) %collective-permute-start.12) | collective-permute-done | bytes 196640 | tf_op jit(solution)/shard_map/ppermute | solution.py:198
  113.3 5.4 %collective-permute-done.14 = bf16[128,768]{1,0:T(8,128)(2,1)S(1)} collective-permute-done((bf16[128,768]{1,0:T(8,128)(2,1)S(1)}, bf16[128,768]{1,0:T(8,128)(2,1)S(1)}, u32[]{:S(2)}, u32[]{:S(2)}) %collective-permute-start.14) | collective-permute-done | bytes 196640 | tf_op jit(solution)/shard_map/ppermute | solution.py:198
  123.5 4.4 %all-to-all-start.1 = ((bf16[192,4,512]{2,0,1:T(8,128)(2,1)}), bf16[192,4,512]{2,0,1:T(8,128)(2,1)}, u32[]{:S(2)}, u32[]{:S(2)}) async-start(bf16[192,4,512]{2,0,1:T(8,128)(2,1)} %bitcast.22), calls=%async_computation.1 | async-start | bytes 1572864 | tf_op jit(solution)/shard_map/all_to_all | solution.py:420
  127.9 3.5 %broadcast_in_dim.22 = bf16[1536,2048]{1,0:T(8,128)(2,1)} broadcast(bf16[]{:T(256)} %constant.237.clone.1), dimensions={} | broadcast | bytes 6291458 | tf_op jit(solution)/shard_map/broadcast_in_dim | solution.py:409
  131.4 2.0 %constant_dynamic-update-slice_fusion.1 = bf16[1536,2048]{1,0:T(8,128)(2,1)} fusion(bf16[1536,2048]{1,0:T(8,128)(2,1)} %broadcast_in_dim.22, bf16[1536,1024]{1,0:T(8,128)(2,1)S(1)} %constant_dynamic-update-slice_fusion.2, s32[]{:T(128)S(6)} %select_n.390), kind=kLoop, calls=%fused_computation.45 | loop fusion | bytes 6291460 | tf_op jit(solution)/shard_map/dynamic_update_slice | solution.py:410
  133.4 6.0 %all-to-all-done.1 = bf16[192,4,512]{2,0,1:T(8,128)(2,1)} async-done(((bf16[192,4,512]{2,0,1:T(8,128)(2,1)}), bf16[192,4,512]{2,0,1:T(8,128)(2,1)}, u32[]{:S(2)}, u32[]{:S(2)}) %all-to-all-start.1) | async-done | bytes 786464 | tf_op jit(solution)/shard_map/all_to_all | solution.py:420
  139.4 2.0 %reduce_sum.12 = bf16[192,512]{1,0:T(8,128)(2,1)} reduce(bf16[192,4,512]{2,0,1:T(8,128)(2,1)} %all-to-all-done.1, bf16[]{:T(256)} %constant.237.clone.1), dimensions={1}, to_apply=%region_0.1 | reduce | flops 294912 | bytes 983042 | tf_op jit(solution)/shard_map/reduce_sum | solution.py:423
  141.4 4.0 %constant_dynamic-update-slice_fusion = bf16[1536,2048]{1,0:T(8,128)(2,1)} fusion(bf16[1536,2048]{1,0:T(8,128)(2,1)} %constant_dynamic-update-slice_fusion.1, bf16[1536,1024]{1,0:T(8,128)(2,1)} %collective-permute-done.22, s32[]{:T(128)S(6)} %select_n.398), kind=kLoop, calls=%fused_computation.44 | loop fusion | bytes 6291460 | tf_op jit(solution)/shard_map/dynamic_update_slice | solution.py:411
  145.4 6.0 %fusion.21 = f32[256,2048]{1,0:T(8,128)} fusion(bf16[256,1536]{1,0:T(8,128)(2,1)S(1)} %copy-done.7, bf16[1536,2048]{1,0:T(8,128)(2,1)} %constant_dynamic-update-slice_fusion), kind=kOutput, calls=%fused_computation.70 | convolution fusion | flops 1610612736 | bytes 9175040 | tf_op jit(solution)/shard_map/dot_general | solution.py:211
  151.4 5.9 %fusion.20 = f32[256,2048]{1,0:T(8,128)} fusion(bf16[256,1536]{1,0:T(8,128)(2,1)S(1)} %copy-done.5, bf16[1536,2048]{1,0:T(8,128)(2,1)} %constant_dynamic-update-slice_fusion), kind=kOutput, calls=%fused_computation.69 | convolution fusion | flops 1610612736 | bytes 9175040 | tf_op jit(solution)/shard_map/dot_general | solution.py:211
  157.3 8.7 %fusion.19 = f32[512,2048]{1,0:T(8,128)} fusion(bf16[512,1536]{1,0:T(8,128)(2,1)} %constant_dynamic-update-slice_fusion.10, bf16[1536,2048]{1,0:T(8,128)(2,1)} %constant_dynamic-update-slice_fusion), kind=kOutput, calls=%fused_computation.68 | convolution fusion | flops 3221225472 | bytes 12058624 | tf_op jit(solution)/shard_map/dot_general | solution.py:211
  (103 shorter events, 45.5 us)
Async XLA Ops:
  2.6 15.1 %collective-permute-start.15 = (bf16[192,1024]{1,0:T(8,128)(2,1)}, bf16[192,1024]{1,0:T(8,128)(2,1)}, u32[]{:S(2)}, u32[]{:S(2)}) collective-permute-start(bf16[192,1024]{1,0:T(8,128)(2,1)} %get-tuple-element.13), channel_id=1, source_target_pairs={{0,8},{8,16},{16,24},{24,28},{28,20},{20,12},{12,4},{4,0},{1,9},{9... | collective-permute-start | bytes 1179656 | tf_op jit(solution)/shard_map/ppermute | solution.py:198
  5.7 14.2 %collective-permute-start.16 = (bf16[192,1024]{1,0:T(8,128)(2,1)}, bf16[192,1024]{1,0:T(8,128)(2,1)}, u32[]{:S(2)}, u32[]{:S(2)}) collective-permute-start(bf16[192,1024]{1,0:T(8,128)(2,1)} %get-tuple-element.13), channel_id=1, source_target_pairs={{8,0},{16,8},{24,16},{28,24},{20,28},{12,20},{4,12},{0,4},{9,1},{1... | collective-permute-start | bytes 1179656 | tf_op jit(solution)/shard_map/ppermute | solution.py:200
  10.6 44.9 %all-to-all-start = ((bf16[8,192,256]{2,1,0:T(8,128)(2,1)}), bf16[8,192,256]{2,1,0:T(8,128)(2,1)}, u32[]{:S(2)}, u32[]{:S(2)}) async-start(bf16[8,192,256]{2,1,0:T(8,128)(2,1)} %project.1), calls=%async_computation | async-start | bytes 1572864 | tf_op jit(solution)/shard_map/all_to_all | solution.py:335
  17.8 20.1 %collective-permute-start.17 = (bf16[192,1024]{1,0:T(8,128)(2,1)}, bf16[192,1024]{1,0:T(8,128)(2,1)}, u32[]{:S(2)}, u32[]{:S(2)}) collective-permute-start(bf16[192,1024]{1,0:T(8,128)(2,1)} %collective-permute-done.15), channel_id=1, source_target_pairs={{0,8},{8,16},{16,24},{24,28},{28,20},{20,12},{12,4},{4,0},{1,9},{9... | collective-permute-start | bytes 1179656 | tf_op jit(solution)/shard_map/ppermute | solution.py:198
  19.8 24.7 %collective-permute-start.18 = (bf16[192,1024]{1,0:T(8,128)(2,1)}, bf16[192,1024]{1,0:T(8,128)(2,1)}, u32[]{:S(2)}, u32[]{:S(2)}) collective-permute-start(bf16[192,1024]{1,0:T(8,128)(2,1)} %collective-permute-done.16), channel_id=1, source_target_pairs={{8,0},{16,8},{24,16},{28,24},{20,28},{12,20},{4,12},{0,4},{9,1},{1... | collective-permute-start | bytes 1179656 | tf_op jit(solution)/shard_map/ppermute | solution.py:200
  37.8 13.7 %collective-permute-start.19 = (bf16[192,1024]{1,0:T(8,128)(2,1)}, bf16[192,1024]{1,0:T(8,128)(2,1)S(1)}, u32[]{:S(2)}, u32[]{:S(2)}) collective-permute-start(bf16[192,1024]{1,0:T(8,128)(2,1)} %collective-permute-done.17), channel_id=1, source_target_pairs={{0,8},{8,16},{16,24},{24,28},{28,20},{20,12},{12,4},{4,0},{1,9},{9... | collective-permute-start | bytes 1179656 | tf_op jit(solution)/shard_map/ppermute | solution.py:198
  44.5 10.9 %collective-permute-start.20 = (bf16[192,1024]{1,0:T(8,128)(2,1)}, bf16[192,1024]{1,0:T(8,128)(2,1)S(1)}, u32[]{:S(2)}, u32[]{:S(2)}) collective-permute-start(bf16[192,1024]{1,0:T(8,128)(2,1)} %collective-permute-done.18), channel_id=1, source_target_pairs={{8,0},{16,8},{24,16},{28,24},{20,28},{12,20},{4,12},{0,4},{9,1},{1... | collective-permute-start | bytes 1179656 | tf_op jit(solution)/shard_map/ppermute | solution.py:200
  51.5 26.6 %collective-permute-start.21 = (bf16[192,1024]{1,0:T(8,128)(2,1)S(1)}, bf16[192,1024]{1,0:T(8,128)(2,1)}, u32[]{:S(2)}, u32[]{:S(2)}) collective-permute-start(bf16[192,1024]{1,0:T(8,128)(2,1)S(1)} %collective-permute-done.19), channel_id=1, source_target_pairs={{0,8},{8,16},{16,24},{24,28},{28,20},{20,12},{12,4},{4,0},{1,9},{9... | collective-permute-start | bytes 1179656 | tf_op jit(solution)/shard_map/ppermute | solution.py:198
  72.0 8.1 %collective-permute-start = (bf16[64,1536]{1,0:T(8,128)(2,1)}, bf16[64,1536]{1,0:T(8,128)(2,1)}, u32[]{:S(2)}, u32[]{:S(2)}) collective-permute-start(bf16[64,1536]{1,0:T(8,128)(2,1)} %get-tuple-element.8), channel_id=1, source_target_pairs={{0,8},{8,16},{16,24},{24,28},{28,20},{20,12},{12,4},{4,0},{1,9},{9... | collective-permute-start | bytes 589832 | tf_op jit(solution)/shard_map/ppermute | solution.py:198
  73.7 7.6 %collective-permute-start.1 = (bf16[64,1536]{1,0:T(8,128)(2,1)}, bf16[64,1536]{1,0:T(8,128)(2,1)}, u32[]{:S(2)}, u32[]{:S(2)}) collective-permute-start(bf16[64,1536]{1,0:T(8,128)(2,1)} %get-tuple-element.8), channel_id=1, source_target_pairs={{8,0},{16,8},{24,16},{28,24},{20,28},{12,20},{4,12},{0,4},{9,1},{1... | collective-permute-start | bytes 589832 | tf_op jit(solution)/shard_map/ppermute | solution.py:200
  75.0 13.1 %collective-permute-start.7 = (f32[128,768]{1,0:T(8,128)S(1)}, f32[128,768]{1,0:T(8,128)S(1)}, u32[]{:S(2)}, u32[]{:S(2)}) collective-permute-start(f32[128,768]{1,0:T(8,128)S(1)} %constant_dynamic-slice_fusion.1), channel_id=1, source_target_pairs={{0,4},{4,0},{8,12},{12,8},{16,20},{20,16},{24,28},{28,24},{1,5},{5... | collective-permute-start | bytes 1179656 | tf_op jit(solution)/shard_map/ppermute | solution.py:371
  79.2 62.2 %collective-permute-start.22 = (bf16[1536,1024]{1,0:T(8,128)(2,1)S(1)}, bf16[1536,1024]{1,0:T(8,128)(2,1)}, u32[]{:S(2)}, u32[]{:S(2)}) collective-permute-start(bf16[1536,1024]{1,0:T(8,128)(2,1)S(1)} %constant_dynamic-update-slice_fusion.2), channel_id=1, source_target_pairs={{0,1},{1,0},{2,3},{3,2},{4,5},{5,4},{6,7},{7,6},{8,9},{9,8},{10,11... | collective-permute-start | bytes 9437192 | tf_op jit(solution)/shard_map/ppermute | solution.py:343
  80.1 13.0 %collective-permute-start.2 = (bf16[64,1536]{1,0:T(8,128)(2,1)}, bf16[64,1536]{1,0:T(8,128)(2,1)S(1)}, u32[]{:S(2)}, u32[]{:S(2)}) collective-permute-start(bf16[64,1536]{1,0:T(8,128)(2,1)} %collective-permute-done), channel_id=1, source_target_pairs={{0,8},{8,16},{16,24},{24,28},{28,20},{20,12},{12,4},{4,0},{1,9},{9... | collective-permute-start | bytes 589832 | tf_op jit(solution)/shard_map/ppermute | solution.py:198
  81.3 12.7 %collective-permute-start.3 = (bf16[64,1536]{1,0:T(8,128)(2,1)}, bf16[64,1536]{1,0:T(8,128)(2,1)S(1)}, u32[]{:S(2)}, u32[]{:S(2)}) collective-permute-start(bf16[64,1536]{1,0:T(8,128)(2,1)} %collective-permute-done.1), channel_id=1, source_target_pairs={{8,0},{16,8},{24,16},{28,24},{20,28},{12,20},{4,12},{0,4},{9,1},{1... | collective-permute-start | bytes 589832 | tf_op jit(solution)/shard_map/ppermute | solution.py:200
  91.0 7.0 %collective-permute-start.8 = (bf16[128,768]{1,0:T(8,128)(2,1)}, bf16[128,768]{1,0:T(8,128)(2,1)S(1)}, u32[]{:S(2)}, u32[]{:S(2)}) collective-permute-start(bf16[128,768]{1,0:T(8,128)(2,1)} %keys.1), channel_id=1, source_target_pairs={{0,8},{8,16},{16,24},{24,28},{28,20},{20,12},{12,4},{4,0},{1,9},{9... | collective-permute-start | bytes 589832 | tf_op jit(solution)/shard_map/ppermute | solution.py:198
  91.0 8.1 %collective-permute-start.9 = (bf16[128,768]{1,0:T(8,128)(2,1)}, bf16[128,768]{1,0:T(8,128)(2,1)S(1)}, u32[]{:S(2)}, u32[]{:S(2)}) collective-permute-start(bf16[128,768]{1,0:T(8,128)(2,1)} %keys.1), channel_id=1, source_target_pairs={{8,0},{16,8},{24,16},{28,24},{20,28},{12,20},{4,12},{0,4},{9,1},{1... | collective-permute-start | bytes 589832 | tf_op jit(solution)/shard_map/ppermute | solution.py:200
  93.0 9.2 %collective-permute-start.4 = (bf16[64,1536]{1,0:T(8,128)(2,1)S(1)}, bf16[64,1536]{1,0:T(8,128)(2,1)S(1)}, u32[]{:S(2)}, u32[]{:S(2)}) collective-permute-start(bf16[64,1536]{1,0:T(8,128)(2,1)S(1)} %collective-permute-done.2), channel_id=1, source_target_pairs={{0,8},{8,16},{16,24},{24,28},{28,20},{20,12},{12,4},{4,0},{1,9},{9... | collective-permute-start | bytes 589832 | tf_op jit(solution)/shard_map/ppermute | solution.py:198
  94.0 10.0 %collective-permute-start.5 = (bf16[64,1536]{1,0:T(8,128)(2,1)S(1)}, bf16[64,1536]{1,0:T(8,128)(2,1)S(1)}, u32[]{:S(2)}, u32[]{:S(2)}) collective-permute-start(bf16[64,1536]{1,0:T(8,128)(2,1)S(1)} %collective-permute-done.3), channel_id=1, source_target_pairs={{8,0},{16,8},{24,16},{28,24},{20,28},{12,20},{4,12},{0,4},{9,1},{1... | collective-permute-start | bytes 589832 | tf_op jit(solution)/shard_map/ppermute | solution.py:200
  98.0 8.4 %collective-permute-start.10 = (bf16[128,768]{1,0:T(8,128)(2,1)S(1)}, bf16[128,768]{1,0:T(8,128)(2,1)S(1)}, u32[]{:S(2)}, u32[]{:S(2)}) collective-permute-start(bf16[128,768]{1,0:T(8,128)(2,1)S(1)} %collective-permute-done.8), channel_id=1, source_target_pairs={{0,8},{8,16},{16,24},{24,28},{28,20},{20,12},{12,4},{4,0},{1,9},{9... | collective-permute-start | bytes 589832 | tf_op jit(solution)/shard_map/ppermute | solution.py:198
  99.1 8.4 %collective-permute-start.11 = (bf16[128,768]{1,0:T(8,128)(2,1)S(1)}, bf16[128,768]{1,0:T(8,128)(2,1)S(1)}, u32[]{:S(2)}, u32[]{:S(2)}) collective-permute-start(bf16[128,768]{1,0:T(8,128)(2,1)S(1)} %collective-permute-done.9), channel_id=1, source_target_pairs={{8,0},{16,8},{24,16},{28,24},{20,28},{12,20},{4,12},{0,4},{9,1},{1... | collective-permute-start | bytes 589832 | tf_op jit(solution)/shard_map/ppermute | solution.py:200
  102.2 7.3 %collective-permute-start.6 = (bf16[64,1536]{1,0:T(8,128)(2,1)S(1)}, bf16[64,1536]{1,0:T(8,128)(2,1)S(1)}, u32[]{:S(2)}, u32[]{:S(2)}) collective-permute-start(bf16[64,1536]{1,0:T(8,128)(2,1)S(1)} %collective-permute-done.4), channel_id=1, source_target_pairs={{0,8},{8,16},{16,24},{24,28},{28,20},{20,12},{12,4},{4,0},{1,9},{9... | collective-permute-start | bytes 589832 | tf_op jit(solution)/shard_map/ppermute | solution.py:198
  106.4 6.6 %collective-permute-start.12 = (bf16[128,768]{1,0:T(8,128)(2,1)S(1)}, bf16[128,768]{1,0:T(8,128)(2,1)S(1)}, u32[]{:S(2)}, u32[]{:S(2)}) collective-permute-start(bf16[128,768]{1,0:T(8,128)(2,1)S(1)} %collective-permute-done.10), channel_id=1, source_target_pairs={{0,8},{8,16},{16,24},{24,28},{28,20},{20,12},{12,4},{4,0},{1,9},{9... | collective-permute-start | bytes 589832 | tf_op jit(solution)/shard_map/ppermute | solution.py:198
  107.5 5.8 %collective-permute-start.13 = (bf16[128,768]{1,0:T(8,128)(2,1)S(1)}, bf16[128,768]{1,0:T(8,128)(2,1)S(1)}, u32[]{:S(2)}, u32[]{:S(2)}) collective-permute-start(bf16[128,768]{1,0:T(8,128)(2,1)S(1)} %collective-permute-done.11), channel_id=1, source_target_pairs={{8,0},{16,8},{24,16},{28,24},{20,28},{12,20},{4,12},{0,4},{9,1},{1... | collective-permute-start | bytes 589832 | tf_op jit(solution)/shard_map/ppermute | solution.py:200
  123.5 15.9 %all-to-all-start.1 = ((bf16[192,4,512]{2,0,1:T(8,128)(2,1)}), bf16[192,4,512]{2,0,1:T(8,128)(2,1)}, u32[]{:S(2)}, u32[]{:S(2)}) async-start(bf16[192,4,512]{2,0,1:T(8,128)(2,1)} %bitcast.22), calls=%async_computation.1 | async-start | bytes 1572864 | tf_op jit(solution)/shard_map/all_to_all | solution.py:420
  (14 other events, 87.2 us)
